TPU v7x, 32 devices: a whole 2x2x4 slice. The times are simulated.
32 devices in a mesh: fs: 16 (over z, y, x), tp: 2 (over core).
Axes of the slice: x: 2, y: 2, z: 4, core: 2. Of those that a mesh axis runs over, the one named last changes fastest.
Arguments:
- x_late: bfloat16 [4096, 2048], P('fs'), may hold values from -6 to 6
- x_early: bfloat16 [4096, 2048], P('fs'), may hold values from -6 to 6
- cotangent: bfloat16 [4096, 2048], P('fs'), may hold values from -6 to 6
- w_gate: bfloat16 [2048, 4096], P('fs', 'tp'), may hold values from -0.125 to 0.125
- w_up: bfloat16 [2048, 4096], P('fs', 'tp'), may hold values from -0.125 to 0.125
- w_down: bfloat16 [4096, 2048], P('tp', 'fs'), may hold values from -0.09375 to 0.09375
- conv_taps: float32 [3, 4096], replicated, may hold values from -3 to 3
- conv_bias: float32 [4096], replicated, may hold values from -3 to 3
- grad_down: float32 [4096, 2048], P('tp', 'fs'), may hold values from -60 to 60
Outputs:
- y_late: bfloat16 [4096, 2048], P('fs')
- dx_early: bfloat16 [4096, 2048], P('fs')
- grad_down_out: float32 [4096, 2048], P('tp', 'fs')
All inputs are finite; a program needn't handle non-finite values.
Results may differ from a plain program's by a relative error of at most 0.017.
Values may be sent and summed in bfloat16 or wider, within the bound.
A program may use at most 128 MiB of HBM per device.

v0:
```python
import jax
import jax.numpy as jnp
from jax import lax
from jax.sharding import PartitionSpec as P


def shift_later(field, steps):
    pad = jnp.zeros((steps, field.shape[1]), jnp.float32)
    return jnp.concatenate([pad, field[: field.shape[0] - steps]], axis=0)


def shift_earlier(field, steps):
    pad = jnp.zeros((steps, field.shape[1]), jnp.float32)
    return jnp.concatenate([field[steps:], pad], axis=0)


def contract_last(left, right):
    return lax.dot_general(
        left, right, (((1,), (1,)), ((), ())), preferred_element_type=jnp.float32
    )


def hidden_parts(inputs, gate_full, up_full, taps, bias):
    gate = (
        jnp.dot(inputs, gate_full, preferred_element_type=jnp.float32)
        .astype(jnp.bfloat16)
        .astype(jnp.float32)
    )
    up = jnp.dot(inputs, up_full, preferred_element_type=jnp.float32)
    conv = bias + taps[2] * gate + taps[1] * shift_later(gate, 1) + taps[0] * shift_later(gate, 2)
    act = jax.nn.silu(conv)
    hidden = (act * up).astype(jnp.bfloat16)
    return (conv, act, up, hidden)


def forward_pass(x_late, gate_full, up_full, down_full, taps, bias):
    conv, act, up, hidden = hidden_parts(x_late, gate_full, up_full, taps, bias)
    partial_value = jnp.dot(hidden, down_full, preferred_element_type=jnp.float32)
    return lax.psum(partial_value.astype(jnp.bfloat16), "tp")


def backward_pass(x_early, cotangent, gate_full, up_full, down_full, taps, bias, grad_down):
    conv, act, up, hidden = hidden_parts(x_early, gate_full, up_full, taps, bias)
    dhidden = contract_last(cotangent, down_full)
    summed = lax.psum_scatter(
        lax.dot_general(
            cotangent, hidden, (((0,), (0,)), ((), ())), preferred_element_type=jnp.float32
        ),
        "fs",
        scatter_dimension=0,
        tiled=True,
    )
    grad_down_out = grad_down + summed.T
    dup = (dhidden * act).astype(jnp.bfloat16)
    sig = jax.nn.sigmoid(conv)
    dconv = dhidden * up * sig * (1.0 + conv * (1.0 - sig))
    dgate = taps[2] * dconv + taps[1] * shift_earlier(dconv, 1) + taps[0] * shift_earlier(dconv, 2)
    dgate = dgate.astype(jnp.bfloat16)
    partial_value = contract_last(dup, up_full) + contract_last(dgate, gate_full)
    dx_early = lax.psum(partial_value.astype(jnp.bfloat16), "tp")
    return (dx_early, grad_down_out)


def shards(x_late, x_early, cotangent, w_gate, w_up, w_down, conv_taps, conv_bias, grad_down):
    width = w_gate.shape[1]
    offset = lax.axis_index("tp") * width
    taps = lax.dynamic_slice_in_dim(conv_taps, offset, width, 1)
    bias = lax.dynamic_slice_in_dim(conv_bias, offset, width, 0)
    gate_full, up_full = (
        lax.all_gather(w_gate, "fs", axis=0, tiled=True),
        lax.all_gather(w_up, "fs", axis=0, tiled=True),
    )
    down_full = lax.all_gather(w_down, "fs", axis=1, tiled=True)
    y_late = forward_pass(x_late, gate_full, up_full, down_full, taps, bias)
    dx_early, grad_down_out = backward_pass(
        x_early, cotangent, gate_full, up_full, down_full, taps, bias, grad_down
    )
    return (y_late, dx_early, grad_down_out)


def solution(mesh):
    placed = (
        P("fs", None),
        P("fs", None),
        P("fs", None),
        P("fs", "tp"),
        P("fs", "tp"),
        P("tp", "fs"),
        P(),
        P(),
        P("tp", "fs"),
    )
    return jax.shard_map(
        shards,
        mesh=mesh,
        in_specs=placed,
        out_specs=(P("fs", None), P("fs", None), P("tp", "fs")),
        check_vma=False,
    )
```

profile of v0, /device:TPU:0, one launch (start us, length us, event | category | flops | bytes accessed | tf_op | source)
XLA Modules:
  0.0 786.5 jit_solution(6254999555990808073)
XLA Ops:
  7.2 0.0 copy-start
  7.2 0.0 all-gather.4.cloned.1.call-start
  7.2 0.7 all-gather.4.cloned.1.call-update
  7.9 0.0 all-gather.6.cloned.1.call-start
  8.0 0.7 all-gather.6.cloned.1.call-update
  8.7 0.0 all-gather.8.cloned.1.call-start
  8.7 0.7 all-gather.8.cloned.1.call-update
  9.4 0.0 reduce-scatter.2.cloned.1.call-start
  9.4 0.7 dynamic_slice.6
  10.2 1.0 fusion.16
  11.1 0.0 copy-start.7
  11.1 114.7 %all-gather.4.cloned.1.call-done = bf16[2048,2048]{1,0:T(8,128)(2,1)} async-done(((bf16[128,2048]{1,0:T(8,128)(2,1)}), bf16[2048,2048]{1,0:T(8,128)(2,1)}) %all-gather.4.cloned.1.call-update) | async-done | bytes 8388624 | tf_op jit(solution)/shard_map/all_gather | solution.py:70
  125.8 7.4 fusion.2
  133.2 105.9 %all-gather.6.cloned.1.call-done = bf16[2048,2048]{1,0:T(8,128)(2,1)} async-done(((bf16[128,2048]{1,0:T(8,128)(2,1)}), bf16[2048,2048]{1,0:T(8,128)(2,1)}) %all-gather.6.cloned.1.call-update) | async-done | bytes 8388624 | tf_op jit(solution)/shard_map/all_gather | solution.py:71
  239.1 0.0 copy-done.7
  239.1 7.1 fusion.17
  246.2 135.7 %all-gather.8.cloned.1.call-done = bf16[2048,2048]{1,0:T(8,128)(2,1)} async-done(((bf16[2048,128]{1,0:T(8,128)(2,1)}), bf16[2048,2048]{1,0:T(8,128)(2,1)}) %all-gather.8.cloned.1.call-update) | async-done | bytes 8388624 | tf_op jit(solution)/shard_map/all_gather | solution.py:73
  381.8 0.0 copy-done
  381.8 0.0 copy-start.4
  381.8 10.6 %add_multiply_fusion = (f32[256,2048]{1,0:T(8,128)S(1)}, f32[256,2048]{1,0:T(8,128)S(1)}, f32[256,2048]{1,0:T(8,128)}) fusion(f32[256,2048]{1,0:T(8,128)} %fusion.17, f32[254,2048]{1,0:T(8,128)} %bitcast.38, f32[2048]{0:T(1024)S(1)} %bitcast.31, f32[255,2048]{1,0:T(8,128)} %bitcast.39, f32[2048]{0:T(1024)S(1)} %bitcast.28, f32[256,2048]{1,0:T(8,128)} %fusion.2, ...), kind=kOutput, calls=%fused_computation.12 | convolution fusion | flops 2155347968 | bytes 24125440 | tf_op jit(solution)/shard_map/dot_general | solution.py:18
  392.5 0.0 copy-start.2
  392.5 1.3 copy-done.2
  393.8 0.0 copy-done.4
  393.8 8.2 %convolution_bitcast_fusion = f32[2048,2048]{0,1:T(8,128)} fusion(bf16[256,2048]{1,0:T(8,128)(2,1)S(1)} %copy-done, f32[256,2048]{1,0:T(8,128)S(1)} %copy-done.4, f32[256,2048]{1,0:T(8,128)S(1)} %get-tuple-element.6), kind=kOutput, calls=%fused_computation | convolution fusion | flops 2150629376 | bytes 22020096 | tf_op jit(solution)/shard_map/dot_general | solution.py:46
  402.0 0.0 reduce-scatter.2.cloned.1.call-update
  402.0 0.2 all-reduce.9.cloned.1.call-start
  402.2 0.0 copy-start.8
  402.2 0.2 slice.47
  402.4 0.0 slice-start
  402.4 0.2 slice.46
  402.6 0.8 copy-done.8
  403.5 0.0 copy-start.3
  403.5 0.0 copy-start.9
  403.5 0.0 slice-start.1
  403.5 8.4 %fusion.3 = f32[256,2048]{1,0:T(8,128)} fusion(bf16[256,2048]{1,0:T(8,128)(2,1)S(1)} %copy-done.8, bf16[2048,2048]{1,0:T(8,128)(2,1)} %all-gather.4.cloned.1.call-done), kind=kOutput, calls=%fused_computation.9 | convolution fusion | flops 2148532224 | bytes 11534336 | tf_op jit(solution)/shard_map/dot_general | solution.py:25
  411.8 0.0 copy-done.3
  411.8 0.0 copy-done.9
  411.8 7.2 fusion.5
  419.0 0.0 slice-done
  419.0 0.0 slice-done.1
  419.0 5.1 fusion
  424.1 13.8 %convolution_convert_fusion.1 = bf16[256,2048]{1,0:T(8,128)(2,1)} fusion(bf16[2048,2048]{1,0:T(8,128)(2,1)} %all-gather.8.cloned.1.call-done, bf16[256,2048]{1,0:T(8,128)(2,1)S(1)} %copy-done.8, bf16[2048,2048]{1,0:T(8,128)(2,1)} %all-gather.6.cloned.1.call-done, f32[254,2048]{1,0:T(8,128)} %bitcast.36, f32[255,2048]{1,0:T(8,128)} %bitcast.37, ...), kind=kOutput, calls=%fused_computation.7 | convolution fusion | flops 4301783040 | bytes 25174016 | tf_op jit(solution)/shard_map/dot_general | solution.py:38
  437.9 0.0 copy-start.5
  437.9 0.0 all-reduce.9.cloned.1.call-update
  437.9 308.8 %reduce-scatter.2.cloned.1.call-done = f32[128,2048]{0,1:T(8,128)} async-done(((f32[2048,2048]{0,1:T(8,128)}), f32[128,2048]{0,1:T(8,128)}) %reduce-scatter.2.cloned.1.call-update) | async-done | bytes 1048592 | tf_op jit(solution)/shard_map/reduce_scatter | solution.py:45
  746.8 0.0 copy-done.5
  746.8 2.3 bitcast_add_fusion
  749.1 27.5 %all-reduce.9.cloned.1.call-done = (bf16[256,2048]{1,0:T(8,128)(2,1)}, bf16[256,2048]{1,0:T(8,128)(2,1)}) async-done(((bf16[256,2048]{1,0:T(8,128)(2,1)}, bf16[256,2048]{1,0:T(8,128)(2,1)}), (bf16[256,2048]{1,0:T(8,128)(2,1)}, bf16[256,2048]{1,0:T(8,128)(2,1)})) %all-reduce.9.cloned.1.call-update) | async-done | bytes 2097168 | tf_op jit(solution)/shard_map/psum | solution.py:39
  776.6 0.0 copy-start.6
  776.6 0.0 copy-start.1
  776.6 2.5 copy.14
  779.0 0.0 copy-done.6
  779.0 1.0 copy.15
  780.0 0.0 copy-done.1
  (1 shorter events, 0.0 us)
Async XLA Ops:
  7.2 374.7 %copy-start = (bf16[256,2048]{1,0:T(8,128)(2,1)S(1)}, bf16[256,2048]{1,0:T(8,128)(2,1)}, u32[]{:S(2)}) copy-start(bf16[256,2048]{1,0:T(8,128)(2,1)} %param.11) | copy-start | bytes 3145732
  7.2 118.6 %all-gather.4.cloned.1.call-start = ((), (), s32[]{:S(2)}) async-start(), calls=%async_computation.1 | async-start | bytes 8912896 | tf_op jit(solution)/shard_map/all_gather | solution.py:70
  7.9 231.2 %all-gather.6.cloned.1.call-start = ((), (), s32[]{:S(2)}) async-start(), calls=%async_computation.2 | async-start | bytes 8912896 | tf_op jit(solution)/shard_map/all_gather | solution.py:71
  8.7 373.2 %all-gather.8.cloned.1.call-start = ((), (), s32[]{:S(2)}) async-start(), calls=%async_computation.3 | async-start | bytes 8912896 | tf_op jit(solution)/shard_map/all_gather | solution.py:73
  9.4 737.4 %reduce-scatter.2.cloned.1.call-start = ((), (), s32[]{:S(2)}) async-start(), calls=%async_computation.4 | async-start | bytes 17825792 | tf_op jit(solution)/shard_map/reduce_scatter | solution.py:45
  11.1 228.0 %copy-start.7 = (bf16[256,2048]{1,0:T(8,128)(2,1)S(1)}, bf16[256,2048]{1,0:T(8,128)(2,1)}, u32[]{:S(2)}) copy-start(bf16[256,2048]{1,0:T(8,128)(2,1)} %param.10) | copy-start | bytes 3145732
  381.8 11.9 %copy-start.4 = (f32[256,2048]{1,0:T(8,128)S(1)}, f32[256,2048]{1,0:T(8,128)}, u32[]{:S(2)}) copy-start(f32[256,2048]{1,0:T(8,128)} %fusion.17) | copy-start | bytes 6291460
  392.5 1.3 copy-start.2
  402.0 374.6 %all-reduce.9.cloned.1.call-start = ((), (), s32[]{:S(2)}) async-start(), calls=%async_computation.5 | async-start | bytes 4194304 | tf_op jit(solution)/shard_map/psum | solution.py:39
  402.2 1.2 copy-start.8
  402.4 16.6 %slice-start = ((s8[8388608]{0:T(1024)(128)(4,1)}), s8[4194304]{0:T(1024)(128)(4,1)S(1)}, s32[]{:S(2)}) async-start(s8[8388608]{0:T(1024)(128)(4,1)} %bitcast.34), calls=%async_computation.6 | async-start | bytes 8388608
  403.5 8.4 %copy-start.3 = (f32[256,2048]{1,0:T(8,128)S(1)}, f32[256,2048]{1,0:T(8,128)}, u32[]{:S(2)}) copy-start(f32[256,2048]{1,0:T(8,128)} %copy-done.2) | copy-start | bytes 6291460
  403.5 8.4 %copy-start.9 = (f32[256,2048]{1,0:T(8,128)S(1)}, f32[256,2048]{1,0:T(8,128)}, u32[]{:S(2)}) copy-start(f32[256,2048]{1,0:T(8,128)} %get-tuple-element.10) | copy-start | bytes 6291460
  403.5 15.5 %slice-start.1 = ((s8[8388608]{0:T(1024)(128)(4,1)}), s8[4194304]{0:T(1024)(128)(4,1)S(1)}, s32[]{:S(2)}) async-start(s8[8388608]{0:T(1024)(128)(4,1)} %bitcast.34), calls=%async_computation.7 | async-start | bytes 8388608
  437.9 308.8 %copy-start.5 = (f32[2048,128]{1,0:T(8,128)S(1)}, f32[2048,128]{1,0:T(8,128)}, u32[]{:S(2)}) copy-start(f32[2048,128]{1,0:T(8,128)} %param.17) | copy-start | bytes 3145732
  776.6 2.5 copy-start.6
  776.6 3.4 copy-start.1
Sparse Core Ops, SparseCore 0:
  10.8 115.0 all-gather.3
  128.6 110.4 all-gather.5
  241.8 139.9 all-gather.7
  402.1 344.5 reduce-scatter.1
  749.6 26.9 all-reduce.8
where the time goes:
time: 787 us
  waiting for transfers between devices  695 us (88%)
  matrix products  67.7 us (9%)
  between operations  13.9 us (2%)
    reduce_scatter x1, waiting for transfers between devices, backward_pass(): lax.psum_scatter(lax.dot_general(cotangent, hidden, (((0,), (0,)), ((), (...  309 us
    all_gather x1, waiting for transfers between devices, shards(): down_full = lax.all_gather(w_down, 'fs', axis=1, tiled=True)  136 us
    all_gather x1, waiting for transfers between devices, shards(): lax.all_gather(w_gate, 'fs', axis=0, tiled=True)  115 us
    all_gather x1, waiting for transfers between devices, shards(): lax.all_gather(w_up, 'fs', axis=0, tiled=True)  106 us
    psum x1, waiting for transfers between devices, forward_pass(): return lax.psum(partial_value.astype(jnp.bfloat16), 'tp')  27.5 us
    dot_general x3, matrix products, contract_last(): lax.dot_general(left, right, (((1,), (1,)), ((), ())), preferred_element_...  22.9 us
    dot_general x2, matrix products, hidden_parts(): jnp.dot(inputs, gate_full, preferred_element_type=jnp.float32)  15.7 us
  transfers between devices with their start and end apart: 5, of which 5 were waited for; matrix products, arithmetic and copies ran while one was open for 7% of the time, Pallas kernels for 0%

commit v1 on v0

--- a/solution.py
+++ b/solution.py
@@ -70,7 +70,7 @@
         lax.all_gather(w_gate, "fs", axis=0, tiled=True),
         lax.all_gather(w_up, "fs", axis=0, tiled=True),
     )
-    down_full = lax.all_gather(w_down, "fs", axis=1, tiled=True)
+    down_full = jnp.concatenate(lax.all_gather(w_down, "fs"), axis=1)
     y_late = forward_pass(x_late, gate_full, up_full, down_full, taps, bias)
     dx_early, grad_down_out = backward_pass(
         x_early, cotangent, gate_full, up_full, down_full, taps, bias, grad_down

time: 787 us -> 758 us (0.963)
  waiting for transfers between devices: 695 us -> 663 us
  local copies, waits for them, and re-layouts: 7.64 us -> 20.6 us
  matrix products: 67.7 us -> 57.5 us
    all_gather x1, waiting for transfers between devices: 136 us -> 115 us  [shards(): down_full = jnp.concatenate(lax.all_gather(w_down, 'fs'), axis=1)]
    all_gather x1, waiting for transfers between devices: 115 us -> 101 us  [shards(): lax.all_gather(w_gate, 'fs', axis=0, tiled=True)]
    reshape x0 -> x1, local copies, waits for them, and re-layouts: none -> 12.5 us  [shards(): down_full = jnp.concatenate(lax.all_gather(w_down, 'fs'), axis=1)]
    dot_general x3, matrix products: 22.9 us -> 14.2 us  [contract_last(): lax.dot_general(left, right, (((1,), (1,)), ((), ())), preferred_element_...]
where the time goes in v1:
time: 758 us
  waiting for transfers between devices  663 us (87%)
  matrix products  57.5 us (8%)
  local copies, waits for them, and re-layouts  20.6 us (3%)
  between operations  13.9 us (2%)
    reduce_scatter x1, waiting for transfers between devices, backward_pass(): lax.psum_scatter(lax.dot_general(cotangent, hidden, (((0,), (0,)), ((), (...  312 us
    all_gather x1, waiting for transfers between devices, shards(): down_full = jnp.concatenate(lax.all_gather(w_down, 'fs'), axis=1)  115 us
    all_gather x1, waiting for transfers between devices, shards(): lax.all_gather(w_up, 'fs', axis=0, tiled=True)  106 us
    all_gather x1, waiting for transfers between devices, shards(): lax.all_gather(w_gate, 'fs', axis=0, tiled=True)  101 us
    psum x1, waiting for transfers between devices, forward_pass(): return lax.psum(partial_value.astype(jnp.bfloat16), 'tp')  27.6 us
    dot_general x2, matrix products, hidden_parts(): jnp.dot(inputs, gate_full, preferred_element_type=jnp.float32)  15.4 us
  transfers between devices with their start and end apart: 5, of which 5 were waited for; matrix products, arithmetic and copies ran while one was open for 7% of the time, Pallas kernels for 0%

profile of v1, /device:TPU:0, one launch (start us, length us, event | category | flops | bytes accessed | tf_op | source)
XLA Modules:
  0.0 757.7 jit_solution(6112805274584227047)
XLA Ops:
  7.2 0.0 copy-start
  7.2 0.0 all-gather.9.cloned.1.call-start
  7.2 0.7 all-gather.9.cloned.1.call-update
  7.9 0.0 all-gather.5.cloned.1.call-start
  8.0 0.7 all-gather.5.cloned.1.call-update
  8.7 0.0 all-gather.7.cloned.1.call-start
  8.7 0.7 all-gather.7.cloned.1.call-update
  9.4 0.0 reduce-scatter.2.cloned.1.call-start
  9.4 0.7 dynamic_slice.6
  10.2 1.0 fusion.16
  11.1 114.7 %all-gather.9.cloned.1.call-done = bf16[32768,128]{1,0:T(8,128)(2,1)} async-done(((bf16[2048,128]{1,0:T(8,128)(2,1)}), bf16[32768,128]{1,0:T(8,128)(2,1)}) %all-gather.9.cloned.1.call-update) | async-done | bytes 8388624 | tf_op jit(solution)/shard_map/all_gather | solution.py:73
  125.8 0.0 copy-start.7
  125.8 12.5 %copy.12 = bf16[2048,16,128]{0,2,1:T(8,128)(2,1)} copy(bf16[2048,16,128]{2,0,1:T(8,128)(2,1)} %bitcast.29) | data formatting | bytes 16777216 | tf_op jit(solution)/shard_map/reshape | solution.py:73
  138.3 100.8 %all-gather.5.cloned.1.call-done = bf16[2048,2048]{1,0:T(8,128)(2,1)} async-done(((bf16[128,2048]{1,0:T(8,128)(2,1)}), bf16[2048,2048]{1,0:T(8,128)(2,1)}) %all-gather.5.cloned.1.call-update) | async-done | bytes 8388624 | tf_op jit(solution)/shard_map/all_gather | solution.py:70
  239.1 0.0 copy-done.7
  239.1 7.1 fusion.2
  246.1 106.2 %all-gather.7.cloned.1.call-done = bf16[2048,2048]{1,0:T(8,128)(2,1)} async-done(((bf16[128,2048]{1,0:T(8,128)(2,1)}), bf16[2048,2048]{1,0:T(8,128)(2,1)}) %all-gather.7.cloned.1.call-update) | async-done | bytes 8388624 | tf_op jit(solution)/shard_map/all_gather | solution.py:71
  352.4 0.0 copy-start.2
  352.4 0.0 copy-start.9
  352.4 5.9 fusion.17
  358.2 0.0 copy-done
  358.2 0.0 copy-done.2
  358.3 0.5 copy-done.9
  358.7 4.9 add_multiply_fusion
  363.6 0.0 copy-start.3
  363.6 1.3 copy-done.3
  364.9 8.2 %convolution_bitcast_fusion = f32[2048,2048]{0,1:T(8,128)} fusion(bf16[256,2048]{1,0:T(8,128)(2,1)S(1)} %copy-done, f32[256,2048]{1,0:T(8,128)S(1)} %fusion.17, f32[256,2048]{1,0:T(8,128)S(1)} %get-tuple-element.6), kind=kOutput, calls=%fused_computation | convolution fusion | flops 2150629376 | bytes 22020096 | tf_op jit(solution)/shard_map/dot_general | solution.py:46
  373.1 0.0 reduce-scatter.2.cloned.1.call-update
  373.2 0.2 all-reduce.9.cloned.1.call-start
  373.4 0.0 copy-start.8
  373.4 0.2 slice.47
  373.6 0.0 slice-start
  373.6 0.2 slice.46
  373.8 0.8 copy-done.8
  374.6 0.0 copy-start.4
  374.6 0.0 copy-start.10
  374.6 0.0 slice-start.1
  374.6 8.4 %fusion.3 = f32[256,2048]{1,0:T(8,128)} fusion(bf16[256,2048]{1,0:T(8,128)(2,1)S(1)} %copy-done.8, bf16[2048,2048]{1,0:T(8,128)(2,1)} %all-gather.5.cloned.1.call-done), kind=kOutput, calls=%fused_computation.9 | convolution fusion | flops 2148532224 | bytes 11534336 | tf_op jit(solution)/shard_map/dot_general | solution.py:25
  383.0 0.0 copy-done.4
  383.0 0.0 copy-done.10
  383.0 5.8 fusion.5
  388.8 0.0 slice-done
  388.8 0.0 slice-done.1
  388.9 3.5 fusion
  392.4 13.8 %convolution_convert_fusion.1 = bf16[256,2048]{1,0:T(8,128)(2,1)} fusion(bf16[2048,2048]{0,1:T(8,128)(2,1)} %bitcast.30, bf16[256,2048]{1,0:T(8,128)(2,1)S(1)} %copy-done.8, bf16[2048,2048]{1,0:T(8,128)(2,1)} %all-gather.7.cloned.1.call-done, f32[254,2048]{1,0:T(8,128)} %bitcast.43, f32[255,2048]{1,0:T(8,128)} %bitcast.44, f32[256,2048]{1,0:T(8,128)} %fusion.3, ...), kind=kOutput, calls=%fused_computation.7 | convolution fusion | flops 4301783040 | bytes 25174016 | tf_op jit(solution)/shard_map/dot_general | solution.py:38
  406.2 0.0 copy-start.5
  406.2 0.0 all-reduce.9.cloned.1.call-update
  406.2 311.7 %reduce-scatter.2.cloned.1.call-done = f32[128,2048]{0,1:T(8,128)} async-done(((f32[2048,2048]{0,1:T(8,128)}), f32[128,2048]{0,1:T(8,128)}) %reduce-scatter.2.cloned.1.call-update) | async-done | bytes 1048592 | tf_op jit(solution)/shard_map/reduce_scatter | solution.py:45
  717.9 0.0 copy-done.5
  717.9 2.3 bitcast_add_fusion
  720.2 27.6 %all-reduce.9.cloned.1.call-done = (bf16[256,2048]{1,0:T(8,128)(2,1)}, bf16[256,2048]{1,0:T(8,128)(2,1)}) async-done(((bf16[256,2048]{1,0:T(8,128)(2,1)}, bf16[256,2048]{1,0:T(8,128)(2,1)}), (bf16[256,2048]{1,0:T(8,128)(2,1)}, bf16[256,2048]{1,0:T(8,128)(2,1)})) %all-reduce.9.cloned.1.call-update) | async-done | bytes 2097168 | tf_op jit(solution)/shard_map/psum | solution.py:39
  747.8 0.0 copy-start.6
  747.8 0.0 copy-start.1
  747.8 2.5 copy.15
  750.2 0.0 copy-done.6
  750.2 1.0 copy.16
  751.2 0.0 copy-done.1
  (1 shorter events, 0.0 us)
Async XLA Ops:
  7.2 351.1 %copy-start = (bf16[256,2048]{1,0:T(8,128)(2,1)S(1)}, bf16[256,2048]{1,0:T(8,128)(2,1)}, u32[]{:S(2)}) copy-start(bf16[256,2048]{1,0:T(8,128)(2,1)} %param.11) | copy-start | bytes 3145732
  7.2 118.6 %all-gather.9.cloned.1.call-start = ((), (), s32[]{:S(2)}) async-start(), calls=%async_computation.4 | async-start | bytes 8912896 | tf_op jit(solution)/shard_map/all_gather | solution.py:73
  7.9 231.2 %all-gather.5.cloned.1.call-start = ((), (), s32[]{:S(2)}) async-start(), calls=%async_computation.1 | async-start | bytes 8912896 | tf_op jit(solution)/shard_map/all_gather | solution.py:70
  8.7 343.7 %all-gather.7.cloned.1.call-start = ((), (), s32[]{:S(2)}) async-start(), calls=%async_computation.2 | async-start | bytes 8912896 | tf_op jit(solution)/shard_map/all_gather | solution.py:71
  9.4 708.5 %reduce-scatter.2.cloned.1.call-start = ((), (), s32[]{:S(2)}) async-start(), calls=%async_computation.3 | async-start | bytes 17825792 | tf_op jit(solution)/shard_map/reduce_scatter | solution.py:45
  125.8 113.3 %copy-start.7 = (bf16[256,2048]{1,0:T(8,128)(2,1)S(1)}, bf16[256,2048]{1,0:T(8,128)(2,1)}, u32[]{:S(2)}) copy-start(bf16[256,2048]{1,0:T(8,128)(2,1)} %param.10) | copy-start | bytes 3145732
  352.4 5.9 copy-start.2
  352.4 6.4 copy-start.9
  363.6 1.3 copy-start.3
  373.2 374.6 %all-reduce.9.cloned.1.call-start = ((), (), s32[]{:S(2)}) async-start(), calls=%async_computation.5 | async-start | bytes 4194304 | tf_op jit(solution)/shard_map/psum | solution.py:39
  373.4 1.2 copy-start.8
  373.6 15.2 %slice-start = ((s8[8388608]{0:T(1024)(128)(4,1)}), s8[4194304]{0:T(1024)(128)(4,1)S(1)}, s32[]{:S(2)}) async-start(s8[8388608]{0:T(1024)(128)(4,1)} %bitcast.41), calls=%async_computation.6 | async-start | bytes 8388608
  374.6 8.4 %copy-start.4 = (f32[256,2048]{1,0:T(8,128)S(1)}, f32[256,2048]{1,0:T(8,128)}, u32[]{:S(2)}) copy-start(f32[256,2048]{1,0:T(8,128)} %copy-done.3) | copy-start | bytes 6291460
  374.6 8.4 %copy-start.10 = (f32[256,2048]{1,0:T(8,128)S(1)}, f32[256,2048]{1,0:T(8,128)}, u32[]{:S(2)}) copy-start(f32[256,2048]{1,0:T(8,128)} %get-tuple-element.10) | copy-start | bytes 6291460
  374.6 14.2 %slice-start.1 = ((s8[8388608]{0:T(1024)(128)(4,1)}), s8[4194304]{0:T(1024)(128)(4,1)S(1)}, s32[]{:S(2)}) async-start(s8[8388608]{0:T(1024)(128)(4,1)} %bitcast.41), calls=%async_computation.7 | async-start | bytes 8388608
  406.2 311.7 %copy-start.5 = (f32[2048,128]{1,0:T(8,128)S(1)}, f32[2048,128]{1,0:T(8,128)}, u32[]{:S(2)}) copy-start(f32[2048,128]{1,0:T(8,128)} %param.17) | copy-start | bytes 3145732
  747.8 2.5 copy-start.6
  747.8 3.4 copy-start.1
Sparse Core Ops, SparseCore 0:
  10.8 115.0 all-gather.8
  128.6 110.4 all-gather.4
  241.9 110.4 all-gather.6
  373.3 344.5 reduce-scatter.1
  720.7 27.0 all-reduce.8
